TPU v7x, 32 devices: a whole 2x2x4 slice. The times are simulated.
32 devices in a mesh: grp: 2 (over y), kv: 4 (over z), tp: 4 (over x, core).
Axes of the slice: x: 2, y: 2, z: 4, core: 2. Of those that a mesh axis runs over, the one named last changes fastest.
Arguments:
- tokens: bfloat16 [256, 4096], P('grp', 'kv'), parts along dimension 0, may hold values from -36 to 36
- span_lengths: int32 [256], P(('grp', 'kv')), parts along dimension 0, may hold values from 1 to 256, 13107 in all
- block_state: float32 [256, 64, 32, 64], P(('grp', 'kv'), 'tp'), parts along dimension 0, may hold values from -96 to 96
- key_cache: bfloat16 [256, 2048, 256], P(('grp', 'kv'), 'tp'), parts along dimension 0, may hold values from -6 to 6
- value_cache: bfloat16 [256, 4096, 256], P(('grp', 'kv'), 'tp'), parts along dimension 0, may hold values from -6 to 6
- decay_cache: float32 [256, 2048, 256], P(('grp', 'kv'), 'tp'), parts along dimension 0, may hold values from -34 to 0, as said below
- attn_gain: float32 [4096], P('kv'), may hold values from 0.1 to 1.9
- query_weight: bfloat16 [4096, 2048], P('kv', 'tp'), may hold values from -0.09375 to 0.09375
- key_weight: bfloat16 [4096, 2048], P('kv', 'tp'), may hold values from -0.09375 to 0.09375
- value_weight: bfloat16 [4096, 4096], P('kv', 'tp'), may hold values from -0.09375 to 0.09375
- gate_weight: bfloat16 [4096, 4096], P('kv', 'tp'), may hold values from -0.09375 to 0.09375
- decay_matrix: bfloat16 [4096, 2048], P('kv', 'tp'), may hold values from -0.09375 to 0.09375
- decay_offset_bias: float32 [2048], P('tp'), may hold values from -1.4 to 6
- head_gain: float32 [64], replicated, may hold values from 0.1 to 1.9
- out_weight: bfloat16 [4096, 4096], P('tp', 'kv'), may hold values from -0.09375 to 0.09375
- mixer_gain: float32 [4096], P('kv'), may hold values from 0.1 to 1.9
- up_weight: bfloat16 [4096, 16384], P('kv', 'tp'), may hold values from -0.09375 to 0.09375
- down_weight: bfloat16 [16384, 4096], P('tp', 'kv'), may hold values from -0.046875 to 0.046875
Outputs:
- layer_out: bfloat16 [256, 4096], P('grp', 'kv'), parts along dimension 0
There are 2 independent parts, one for each index of `grp`. A program takes and returns all parts, laid end to end along the dimension named above; an argument that names none is the same for every part. Nothing has to cross between parts.
Inputs may be any that keep to these rules, and one draw needn't show every extreme that they name: Cached positions at index span_lengths - 1 and beyond are unused. `decay_cache`: Non-increasing along positions.
All inputs are finite; a program needn't handle non-finite values. No bound on the sum of `span_lengths` on one device may be relied on, other than what follows from the above.
Results may differ from a plain program's by a relative error of at most 0.005.
The roundings to bfloat16 on the way count: a program that leaves them out, or rounds other values in their place, can miss the bound.
Values may be sent and summed in bfloat16 or wider, within the bound.
A program may use at most 128 MiB of HBM per device.

v0:
```python
import jax
import jax.numpy as jnp
from jax import lax
from jax.sharding import PartitionSpec as P

D = 4096
KEY_WIDTH = 32
DV = 64
NORM_EPS = 1e-06
DECAY_SOFTNESS = 16.0


def shards(
    tokens,
    span_lengths,
    block_state,
    key_cache,
    value_cache,
    decay_cache,
    attn_gain,
    query_weight,
    key_weight,
    value_weight,
    gate_weight,
    decay_matrix,
    decay_offset_bias,
    head_gain,
    out_weight,
    mixer_gain,
    up_weight,
    down_weight,
):
    seq_count = block_state.shape[0]
    head_count = block_state.shape[1]
    span_size = key_cache.shape[2]
    whole_rows = tokens.astype(jnp.float32)
    square_sum = jnp.sum(whole_rows * whole_rows, axis=1)
    scaled = (whole_rows * attn_gain).astype(jnp.bfloat16)
    query_part = jnp.dot(scaled, query_weight, preferred_element_type=jnp.float32)
    key_part = jnp.dot(scaled, key_weight, preferred_element_type=jnp.float32)
    value_part = jnp.dot(scaled, value_weight, preferred_element_type=jnp.float32)
    gate_part = jnp.dot(scaled, gate_weight, preferred_element_type=jnp.float32)
    decay_part = jnp.dot(scaled, decay_matrix, preferred_element_type=jnp.float32)
    square_total = lax.psum(square_sum, "kv")
    query_sum, key_sum, value_sum, gate_sum, decay_running_sum = (
        lax.psum_scatter(query_part, "kv", scatter_dimension=0, tiled=True),
        lax.psum_scatter(key_part, "kv", scatter_dimension=0, tiled=True),
        lax.psum_scatter(value_part, "kv", scatter_dimension=0, tiled=True),
        lax.psum_scatter(gate_part, "kv", scatter_dimension=0, tiled=True),
        lax.psum_scatter(decay_part, "kv", scatter_dimension=0, tiled=True),
    )
    own_square = lax.dynamic_slice_in_dim(square_total, lax.axis_index("kv") * seq_count, seq_count)
    scale_per_row = lax.rsqrt(own_square / D + NORM_EPS)[:, None]
    query = (query_sum * scale_per_row * KEY_WIDTH ** (-0.5)).reshape(
        seq_count, head_count, KEY_WIDTH
    )
    key_new = (key_sum * scale_per_row).reshape(seq_count, head_count, KEY_WIDTH)
    value_new = (value_sum * scale_per_row).reshape(seq_count, head_count, DV)
    gate = gate_sum * scale_per_row
    logarithm_decay = (
        jax.nn.log_sigmoid(decay_running_sum * scale_per_row + decay_offset_bias) / DECAY_SOFTNESS
    )
    token_place = lax.broadcasted_iota(jnp.int32, (1, 1, span_size), 2)
    lengths_now = span_lengths[:, None, None]
    previous = jnp.sum(jnp.where(token_place == lengths_now - 2, decay_cache, 0.0), axis=-1)
    now_decay = (previous + logarithm_decay).reshape(seq_count, head_count, KEY_WIDTH)
    decays_span = decay_cache.reshape(seq_count, head_count, KEY_WIDTH, span_size)
    in_use = (token_place < lengths_now - 1)[:, :, None, :]
    factor = jnp.where(in_use, jnp.exp(now_decay[..., None] - decays_span), 0.0)
    keys_span = key_cache.reshape(seq_count, head_count, KEY_WIDTH, span_size)
    scores = jnp.sum(query[..., None] * keys_span.astype(jnp.float32) * factor, axis=2)
    scores_low = scores.astype(jnp.bfloat16)
    values_span = value_cache.reshape(seq_count, head_count, DV, span_size)
    history = jnp.einsum(
        "nhs,nhvs->nhv", scores_low, values_span, preferred_element_type=jnp.float32
    )
    carried = jnp.einsum(
        "nhc,nhcv->nhv", query * jnp.exp(now_decay), block_state, precision=lax.Precision.HIGHEST
    )
    own_term = jnp.sum(query * key_new, axis=-1, keepdims=True) * value_new
    raw = carried + history + own_term
    normed = raw * lax.rsqrt(jnp.mean(raw * raw, axis=-1, keepdims=True) + NORM_EPS) * head_gain
    mixed = (normed.reshape(seq_count, head_count * DV) * jax.nn.silu(gate)).astype(jnp.bfloat16)
    attn_terms = jnp.dot(
        lax.all_gather(mixed, "kv", axis=0, tiled=True),
        out_weight,
        preferred_element_type=jnp.float32,
    )
    attn_out = lax.psum(attn_terms, "tp")
    resid = (whole_rows + attn_out).astype(jnp.bfloat16)
    resid_rows = resid.astype(jnp.float32)
    mixer_square = jnp.sum(resid_rows * resid_rows, axis=1)
    mixer_scaled = (resid_rows * mixer_gain).astype(jnp.bfloat16)
    up_part = jnp.dot(mixer_scaled, up_weight, preferred_element_type=jnp.float32)
    up_share, square_share = (
        lax.psum_scatter(up_part, "kv", scatter_dimension=0, tiled=True),
        lax.psum_scatter(mixer_square, "kv", scatter_dimension=0, tiled=True),
    )
    hidden_share = jnp.square(
        jax.nn.relu(up_share * lax.rsqrt(square_share / D + NORM_EPS)[:, None])
    )
    hidden_share = hidden_share.astype(jnp.bfloat16)
    down_terms = jnp.dot(
        lax.all_gather(hidden_share, "kv", axis=0, tiled=True),
        down_weight,
        preferred_element_type=jnp.float32,
    )
    mixer_out = lax.psum(down_terms, "tp")
    return (resid_rows + mixer_out).astype(jnp.bfloat16)


def solution(mesh):
    placed = (
        P("grp", "kv"),
        P(("grp", "kv")),
        P(("grp", "kv"), "tp", None, None),
        P(("grp", "kv"), "tp", None),
        P(("grp", "kv"), "tp", None),
        P(("grp", "kv"), "tp", None),
        P("kv"),
        P("kv", "tp"),
        P("kv", "tp"),
        P("kv", "tp"),
        P("kv", "tp"),
        P("kv", "tp"),
        P("tp"),
        P(),
        P("tp", "kv"),
        P("kv"),
        P("kv", "tp"),
        P("tp", "kv"),
    )
    return jax.shard_map(
        shards, mesh=mesh, in_specs=placed, out_specs=P("grp", "kv"), check_vma=False
    )
```

profile of v0, /device:TPU:0, one launch (start us, length us, event | category | flops | bytes accessed | tf_op | source)
XLA Modules:
  0.0 293.3 jit_solution(13781271329002494492)
XLA Ops:
  6.5 0.0 reduce-scatter.7.cloned.1.call-start
  6.6 2.5 fusion.21
  9.1 0.0 reduce-scatter.7.cloned.1.call-update
  9.1 0.0 reduce-scatter.11.cloned.1.call-start
  9.2 2.4 fusion.17
  11.5 0.0 reduce-scatter.11.cloned.1.call-update
  11.5 0.0 reduce-scatter.9.cloned.1.call-start
  11.6 2.3 fusion.19
  13.9 0.0 reduce-scatter.9.cloned.1.call-update
  14.0 0.0 reduce-scatter.13.cloned.1.call-start
  14.0 2.2 fusion.15
  16.2 0.0 reduce-scatter.13.cloned.1.call-update
  16.2 0.0 reduce-scatter.15.cloned.1.call-start
  16.3 2.9 fusion.13
  19.2 0.0 reduce-scatter.15.cloned.1.call-update
  19.2 0.0 all-reduce.4.cloned.1.call-start
  19.2 0.1 fusion.3
  19.4 13.6 %psum.21 = f32[128]{0:T(128)S(1)} all-reduce(f32[128]{0:T(128)S(1)} %fusion.3), channel_id=1, replica_groups=mesh['grp'=2,'kv'=4,'tp'=4] {'kv'}, use_global_device_ids=true, to_apply=%region_2.0 | all-reduce | flops 128 | bytes 1024 | tf_op jit(solution)/shard_map/psum | solution.py:44
  33.0 0.1 iota_compare_fusion
  33.0 0.1 iota_compare_fusion.1
  33.1 0.1 add_rsqrt_fusion.1
  33.2 8.0 %select_reduce_fusion = f32[32,512]{1,0:T(8,128)S(1)} fusion(f32[32,512,256]{2,1,0:T(8,128)} %param.23, pred[32,256]{1,0:T(8,128)(4,1)S(1)} %iota_compare_fusion.1), kind=kLoop, calls=%fused_computation.3 | loop fusion | flops 8372224 | bytes 16850944 | tf_op jit(solution)/shard_map/reduce_sum | solution.py:65
  41.2 0.0 reduce-scatter.7.cloned.1.call-done
  41.3 11.6 %reduce-scatter.11.cloned.1.call-done = f32[32,512]{1,0:T(8,128)} async-done(((f32[128,512]{1,0:T(8,128)}), f32[32,512]{1,0:T(8,128)}) %reduce-scatter.11.cloned.1.call-update) | async-done | bytes 65552 | tf_op jit(solution)/shard_map/reduce_scatter | solution.py:47
  52.9 20.5 %reduce-scatter.9.cloned.1.call-done = f32[32,512]{1,0:T(8,128)} async-done(((f32[128,512]{1,0:T(8,128)}), f32[32,512]{1,0:T(8,128)}) %reduce-scatter.9.cloned.1.call-update) | async-done | bytes 65552 | tf_op jit(solution)/shard_map/reduce_scatter | solution.py:50
  73.5 1.0 fusion.25
  74.5 0.1 reshape.83
  74.6 0.1 reshape.82
  74.7 0.1 reshape.86
  74.8 0.1 exponential_multiply_fusion
  75.0 9.7 %fusion.1 = bf16[32,16,256]{2,1,0:T(8,128)(2,1)S(1)} fusion(f32[32,16,32]{2,1,0:T(8,128)S(1)} %reshape.83, f32[32,16,32]{2,1,0:T(8,128)S(1)} %reshape.82, pred[32,256]{1,0:T(8,128)(4,1)S(1)} %iota_compare_fusion, bf16[32,512,256]{2,1,0:T(8,128)(2,1)} %param.21, f32[32,512,256]{2,1,0:T(8,128)} %param.23), kind=kLoop, calls=%fused_computation.2 | loop fusion | flops 25034752 | bytes 25567232 | tf_op jit(solution)/shard_map/reduce_sum | solution.py:71
  84.7 10.3 %fusion.8 = f32[32,16,1,64]{3,2,1,0:T(1,128)S(1)} fusion(bf16[32,16,64,256]{3,2,1,0:T(8,128)(2,1)} %bitcast.34, bf16[32,16,256,1]{2,1,0,3:T(8,128)(2,1)S(1)} %bitcast.32), kind=kOutput, calls=%fused_computation.16 | convolution fusion | flops 16777216 | bytes 17170432 | tf_op jit(solution)/shard_map/nhs,nhvs->nhv/dot_general | solution.py:74
  94.9 9.2 %fusion.29 = f32[32,16,1,64]{3,2,1,0:T(1,128)S(1)} fusion(f32[32,16,32,1]{2,3,1,0:T(1,128)S(1)} %bitcast.31, f32[32,16,32,64]{3,2,1,0:T(8,128)} %param.20), kind=kOutput, calls=%fused_computation.49 | convolution fusion | flops 12582912 | bytes 4390912 | tf_op jit(solution)/shard_map/nhc,nhcv->nhv/dot_general | solution.py:77
  104.2 0.0 reduce-scatter.13.cloned.1.call-done
  104.2 1.0 broadcast_multiply_fusion
  105.2 0.1 reshape.87
  105.3 0.2 multiply_reduce_fusion
  105.6 0.1 multiply_multiply_fusion
  105.7 0.1 reshape.88
  105.8 12.1 %reduce-scatter.15.cloned.1.call-done = f32[32,1024]{1,0:T(8,128)} async-done(((f32[128,1024]{1,0:T(8,128)}), f32[32,1024]{1,0:T(8,128)}) %reduce-scatter.15.cloned.1.call-update) | async-done | bytes 131088 | tf_op jit(solution)/shard_map/reduce_scatter | solution.py:49
  118.0 1.0 multiply_convert_fusion.1
  119.0 13.8 %all_gather.6 = bf16[128,1024]{1,0:T(8,128)(2,1)S(1)} all-gather(bf16[32,1024]{1,0:T(8,128)(2,1)S(1)} %multiply_convert_fusion.1), channel_id=1, replica_groups=mesh['grp'=2,'kv'=4,'tp'=4] {'kv'}, dimensions={0}, use_global_device_ids=true | all-gather | bytes 327680 | tf_op jit(solution)/shard_map/all_gather | solution.py:85
  132.8 1.3 fusion.30
  134.0 0.0 all-reduce.4.cloned.1.call-update
  134.1 0.2 reduce-scatter.17.cloned.1.call-start
  134.3 31.5 %all-reduce.4.cloned.1.call-done = f32[128,1024]{1,0:T(8,128)} async-done(((f32[128,1024]{1,0:T(8,128)}), f32[128,1024]{1,0:T(8,128)}) %all-reduce.4.cloned.1.call-update) | async-done | bytes 524304 | tf_op jit(solution)/shard_map/psum | solution.py:89
  165.8 1.2 fusion.6
  167.0 0.0 copy-start.9
  167.0 6.0 %fusion.10 = f32[128,4096]{1,0:T(8,128)} fusion(bf16[1024,4096]{1,0:T(8,128)(2,1)} %param.34, bf16[128,1024]{1,0:T(8,128)(2,1)S(1)} %get-tuple-element.6, f32[1024]{0:T(1024)S(1)} %copy-done.5), kind=kOutput, calls=%fused_computation.19 | convolution fusion | flops 1074135040 | bytes 10752000 | tf_op jit(solution)/shard_map/dot_general | solution.py:94
  173.0 0.0 reduce-scatter.17.cloned.1.call-update
  173.1 0.0 all-gather.2.cloned.1.call-start
  173.1 0.6 dynamic-slice
  174.4 12.1 %all-reduce = f32[128]{0:T(128)S(1)} all-reduce(f32[128]{0:T(128)S(1)} %get-tuple-element.5), channel_id=8, replica_groups=mesh['grp'=2,'kv'=4,'tp'=4] {'kv'}, use_global_device_ids=true, to_apply=%region_14.15.clone | all-reduce | flops 128 | bytes 1024
  186.4 0.1 fusion.27
  186.5 30.4 %reduce-scatter.17.cloned.1.call-done = f32[32,4096]{1,0:T(8,128)} async-done(((f32[128,4096]{1,0:T(8,128)}), f32[32,4096]{1,0:T(8,128)}) %reduce-scatter.17.cloned.1.call-update) | async-done | bytes 524304 | tf_op jit(solution)/shard_map/reduce_scatter | solution.py:96
  217.0 1.9 multiply_convert_fusion
  218.8 0.0 all-gather.2.cloned.1.call-update
  218.9 0.0 copy-start.1
  218.9 0.0 all-reduce.6.cloned.1.call-start
  218.9 27.3 %all-gather.2.cloned.1.call-done = bf16[128,4096]{1,0:T(8,128)(2,1)} async-done(((bf16[32,4096]{1,0:T(8,128)(2,1)}), bf16[128,4096]{1,0:T(8,128)(2,1)}) %all-gather.2.cloned.1.call-update) | async-done | bytes 1048592 | tf_op jit(solution)/shard_map/all_gather | solution.py:104
  246.2 5.8 %fusion.31 = f32[128,1024]{1,0:T(8,128)} fusion(bf16[128,4096]{1,0:T(8,128)(2,1)} %all-gather.2.cloned.1.call-done, bf16[4096,1024]{1,0:T(8,128)(2,1)} %param.35), kind=kOutput, calls=%fused_computation.51 | convolution fusion | flops 1073741824 | bytes 9961472 | tf_op jit(solution)/shard_map/dot_general | solution.py:103
  252.0 0.0 all-reduce.6.cloned.1.call-update
  252.0 32.9 %all-reduce.6.cloned.1.call-done = f32[128,1024]{1,0:T(8,128)} async-done(((f32[128,1024]{1,0:T(8,128)}), f32[128,1024]{1,0:T(8,128)}) %all-reduce.6.cloned.1.call-update) | async-done | bytes 524304 | tf_op jit(solution)/shard_map/psum | solution.py:108
  284.9 1.8 fusion.7
  (20 shorter events, 0.0 us)
Async XLA Ops:
  6.5 7.5 %copy-start = (bf16[1024,1024]{1,0:T(8,128)(2,1)S(1)}, bf16[1024,1024]{1,0:T(8,128)(2,1)}, u32[]{:S(2)}) copy-start(bf16[1024,1024]{1,0:T(8,128)(2,1)} %param.27) | copy-start | bytes 6291460
  6.5 9.8 %copy-start.2 = (bf16[128,1024]{1,0:T(8,128)(2,1)S(1)}, bf16[128,1024]{1,0:T(8,128)(2,1)}, u32[]{:S(2)}) copy-start(bf16[128,1024]{1,0:T(8,128)(2,1)} %param.18) | copy-start | bytes 786436
  6.5 9.8 %copy-start.4 = (f32[1024]{0:T(1024)S(1)}, f32[1024]{0:T(1024)}, u32[]{:S(2)}) copy-start(f32[1024]{0:T(1024)} %param.24) | copy-start | bytes 12292
  6.5 26.4 %copy-start.8 = (s32[32]{0:T(128)S(1)}, s32[32]{0:T(128)}, u32[]{:S(2)}) copy-start(s32[32]{0:T(128)} %param.19) | copy-start | bytes 388
  6.5 34.7 %reduce-scatter.7.cloned.1.call-start = ((), (), s32[]{:S(2)}) async-start(), calls=%async_computation.6 | async-start | bytes 327680 | tf_op jit(solution)/shard_map/reduce_scatter | solution.py:46
  9.1 43.8 %reduce-scatter.11.cloned.1.call-start = ((), (), s32[]{:S(2)}) async-start(), calls=%async_computation.8 | async-start | bytes 327680 | tf_op jit(solution)/shard_map/reduce_scatter | solution.py:47
  11.5 61.9 %reduce-scatter.9.cloned.1.call-start = ((), (), s32[]{:S(2)}) async-start(), calls=%async_computation.7 | async-start | bytes 327680 | tf_op jit(solution)/shard_map/reduce_scatter | solution.py:50
  14.0 90.2 %reduce-scatter.13.cloned.1.call-start = ((), (), s32[]{:S(2)}) async-start(), calls=%async_computation.9 | async-start | bytes 655360 | tf_op jit(solution)/shard_map/reduce_scatter | solution.py:48
  16.2 101.7 %reduce-scatter.15.cloned.1.call-start = ((), (), s32[]{:S(2)}) async-start(), calls=%async_computation.10 | async-start | bytes 655360 | tf_op jit(solution)/shard_map/reduce_scatter | solution.py:49
  19.2 146.6 %all-reduce.4.cloned.1.call-start = ((), (), s32[]{:S(2)}) async-start(), calls=%async_computation.11 | async-start | bytes 1048576 | tf_op jit(solution)/shard_map/psum | solution.py:89
  33.2 40.2 %copy-start.6 = (f32[512]{0:T(512)S(1)}, f32[512]{0:T(512)}, u32[]{:S(2)}) copy-start(f32[512]{0:T(512)} %param.30) | copy-start | bytes 6148
  94.9 10.6 %copy-start.7 = (f32[64]{0:T(128)S(1)}, f32[64]{0:T(128)}, u32[]{:S(2)}) copy-start(f32[64]{0:T(128)} %param.31) | copy-start | bytes 772
  94.9 37.9 %copy-start.3 = (bf16[1024,1024]{1,0:T(8,128)(2,1)S(1)}, bf16[1024,1024]{1,0:T(8,128)(2,1)}, u32[]{:S(2)}) copy-start(bf16[1024,1024]{1,0:T(8,128)(2,1)} %param.32) | copy-start | bytes 6291460
  94.9 72.1 %copy-start.5 = (f32[1024]{0:T(1024)S(1)}, f32[1024]{0:T(1024)}, u32[]{:S(2)}) copy-start(f32[1024]{0:T(1024)} %param.33) | copy-start | bytes 12292
  134.1 82.9 %reduce-scatter.17.cloned.1.call-start = ((), (), s32[]{:S(2)}) async-start(), calls=%async_computation.12 | async-start | bytes 2621440 | tf_op jit(solution)/shard_map/reduce_scatter | solution.py:96
  167.0 6.1 %copy-start.9 = (u32[32]{0:T(128)S(1)}, u32[32]{0:T(128)}, u32[]{:S(2)}) copy-start(u32[32]{0:T(128)} %constant.44) | copy-start | bytes 388
  173.1 73.1 %all-gather.2.cloned.1.call-start = ((), (), s32[]{:S(2)}) async-start(), calls=%async_computation.13 | async-start | bytes 1310720 | tf_op jit(solution)/shard_map/all_gather | solution.py:104
  218.9 67.9 %copy-start.1 = (bf16[1024,1024]{1,0:T(8,128)(2,1)S(1)}, bf16[1024,1024]{1,0:T(8,128)(2,1)}, u32[]{:S(2)}) copy-start(bf16[1024,1024]{1,0:T(8,128)(2,1)} %param.27) | copy-start | bytes 6291460
  218.9 66.1 %all-reduce.6.cloned.1.call-start = ((), (), s32[]{:S(2)}) async-start(), calls=%async_computation.14 | async-start | bytes 1048576 | tf_op jit(solution)/shard_map/psum | solution.py:108
Sparse Core Ops, SparseCore 0:
  9.6 22.7 reduce-scatter.6
  34.6 18.2 reduce-scatter.10
  55.2 18.2 reduce-scatter.8
  75.6 20.1 reduce-scatter.12
  97.8 20.0 reduce-scatter.14
  134.2 31.5 all-reduce.3
  173.2 43.7 reduce-scatter.16
  219.0 27.1 all-gather.1
  252.1 32.7 all-reduce.5
where the time goes:
time: 294 us; the launch traced here: 293 us
  waiting for transfers between devices  167 us (57%)
  matrix products  44.8 us (15%)
  blocking collectives  39.5 us (13%)
  other arithmetic  26.6 us (9%)
  between operations  14 us (5%)
    psum x1, waiting for transfers between devices, shards(): mixer_out = lax.psum(down_terms, 'tp')  32.9 us
    psum x1, waiting for transfers between devices, shards(): attn_out = lax.psum(attn_terms, 'tp')  31.5 us
    reduce_scatter x1, waiting for transfers between devices, shards(): lax.psum_scatter(up_part, 'kv', scatter_dimension=0, tiled=True)  30.4 us
    all_gather x1, waiting for transfers between devices, shards(): lax.all_gather(hidden_share, 'kv', axis=0, tiled=True)  27.3 us
    reduce_scatter x1, waiting for transfers between devices, shards(): lax.psum_scatter(decay_part, 'kv', scatter_dimension=0, tiled=True)  20.5 us
    all_gather x1, blocking collectives, shards(): lax.all_gather(mixed, 'kv', axis=0, tiled=True)  13.8 us
    psum x1, blocking collectives, shards(): square_total = lax.psum(square_sum, 'kv')  13.6 us
    reduce_scatter x1, waiting for transfers between devices, shards(): lax.psum_scatter(gate_part, 'kv', scatter_dimension=0, tiled=True)  12.1 us
  transfers between devices with their start and end apart: 9, of which 7 were waited for; matrix products, arithmetic and copies ran while one was open for 17% of the time, Pallas kernels for 0%

commit v1 on v0

--- a/solution.py
+++ b/solution.py
@@ -8,6 +8,15 @@
 DV = 64
 NORM_EPS = 1e-06
 DECAY_SOFTNESS = 16.0
+
+
+def added_up(x, axis):
+    size = lax.axis_size(axis)
+    acc, hop = (x, 1)
+    while hop < size:
+        acc = acc + lax.ppermute(acc, axis, [(i, i ^ hop) for i in range(size)])
+        hop = 2 * hop
+    return acc
 
 
 def shards(
@@ -86,7 +95,7 @@
         out_weight,
         preferred_element_type=jnp.float32,
     )
-    attn_out = lax.psum(attn_terms, "tp")
+    attn_out = added_up(attn_terms, "tp")
     resid = (whole_rows + attn_out).astype(jnp.bfloat16)
     resid_rows = resid.astype(jnp.float32)
     mixer_square = jnp.sum(resid_rows * resid_rows, axis=1)

time: 294 us -> 275 us (0.935)
  waiting for transfers between devices: 167 us -> 151 us
  blocking collectives: 39.5 us -> 36.5 us
    psum x1 -> x0, waiting for transfers between devices: 31.5 us -> none  [shards(): attn_out = lax.psum(attn_terms, 'tp')]
    ppermute x0 -> x2, waiting for transfers between devices: none -> 14.4 us  [added_up(): acc = acc + lax.ppermute(acc, axis, [(i, i ^ hop) for i in range(size)])]
    unnamed x1, blocking collectives: 12.1 us -> 8.98 us
  transfers between devices with their start and end apart: 9 -> 10, of which waited for: 7 -> 8; matrix products, arithmetic and copies ran while one was open for 17% -> 19% of each run, Pallas kernels for 0% -> 0%
where the time goes in v1:
time: 275 us; the launch traced here: 274 us
  waiting for transfers between devices  151 us (55%)
  matrix products  44 us (16%)
  blocking collectives  36.5 us (13%)
  other arithmetic  25.6 us (9%)
  between operations  14.4 us (5%)
    psum x1, waiting for transfers between devices, shards(): mixer_out = lax.psum(down_terms, 'tp')  32.9 us
    reduce_scatter x1, waiting for transfers between devices, shards(): lax.psum_scatter(up_part, 'kv', scatter_dimension=0, tiled=True)  31.6 us
    all_gather x1, waiting for transfers between devices, shards(): lax.all_gather(hidden_share, 'kv', axis=0, tiled=True)  27.3 us
    reduce_scatter x1, waiting for transfers between devices, shards(): lax.psum_scatter(decay_part, 'kv', scatter_dimension=0, tiled=True)  20.5 us
    ppermute x2, waiting for transfers between devices, added_up(): acc = acc + lax.ppermute(acc, axis, [(i, i ^ hop) for i in range(size)])  14.4 us
    all_gather x1, blocking collectives, shards(): lax.all_gather(mixed, 'kv', axis=0, tiled=True)  14 us
    psum x1, blocking collectives, shards(): square_total = lax.psum(square_sum, 'kv')  13.6 us
    reduce_scatter x1, waiting for transfers between devices, shards(): lax.psum_scatter(gate_part, 'kv', scatter_dimension=0, tiled=True)  12.1 us
  transfers between devices with their start and end apart: 10, of which 8 were waited for; matrix products, arithmetic and copies ran while one was open for 19% of the time, Pallas kernels for 0%

profile of v1, /device:TPU:0, one launch (start us, length us, event | category | flops | bytes accessed | tf_op | source)
XLA Modules:
  0.0 274.3 jit_solution(16540201385664376728)
XLA Ops:
  6.5 0.0 reduce-scatter.7.cloned.1.call-start
  6.6 2.5 fusion.21
  9.1 0.0 reduce-scatter.7.cloned.1.call-update
  9.1 0.0 reduce-scatter.11.cloned.1.call-start
  9.2 2.4 fusion.17
  11.5 0.0 reduce-scatter.11.cloned.1.call-update
  11.5 0.0 reduce-scatter.9.cloned.1.call-start
  11.6 2.3 fusion.19
  13.9 0.0 reduce-scatter.9.cloned.1.call-update
  14.0 0.0 reduce-scatter.13.cloned.1.call-start
  14.0 2.2 fusion.15
  16.2 0.0 reduce-scatter.13.cloned.1.call-update
  16.2 0.0 reduce-scatter.15.cloned.1.call-start
  16.3 2.9 %fusion.13 = f32[128,1024]{1,0:T(8,128)} fusion(bf16[1024,1024]{1,0:T(8,128)(2,1)} %param.28, bf16[128,1024]{1,0:T(8,128)(2,1)S(1)} %copy-done.2, f32[1024]{0:T(1024)S(1)} %copy-done.4), kind=kOutput, calls=%fused_computation.29 | convolution fusion | flops 268828672 | bytes 2887680 | tf_op jit(solution)/shard_map/dot_general | solution.py:51
  19.2 0.0 reduce-scatter.15.cloned.1.call-update
  19.2 0.0 reduce-scatter.17.cloned.1.call-start
  19.2 0.1 fusion.3
  19.4 13.6 %psum.14 = f32[128]{0:T(128)S(1)} all-reduce(f32[128]{0:T(128)S(1)} %fusion.3), channel_id=1, replica_groups=mesh['grp'=2,'kv'=4,'tp'=4] {'kv'}, use_global_device_ids=true, to_apply=%region_2.0 | all-reduce | flops 128 | bytes 1024 | tf_op jit(solution)/shard_map/psum | solution.py:53
  33.0 0.1 iota_compare_fusion
  33.0 0.1 iota_compare_fusion.1
  33.1 0.1 add_rsqrt_fusion.1
  33.2 8.0 %select_reduce_fusion = f32[32,512]{1,0:T(8,128)S(1)} fusion(f32[32,512,256]{2,1,0:T(8,128)} %param.23, pred[32,256]{1,0:T(8,128)(4,1)S(1)} %iota_compare_fusion.1), kind=kLoop, calls=%fused_computation.3 | loop fusion | flops 8372224 | bytes 16850944 | tf_op jit(solution)/shard_map/reduce_sum | solution.py:74
  41.2 0.0 reduce-scatter.7.cloned.1.call-done
  41.3 11.6 %reduce-scatter.11.cloned.1.call-done = f32[32,512]{1,0:T(8,128)} async-done(((f32[128,512]{1,0:T(8,128)}), f32[32,512]{1,0:T(8,128)}) %reduce-scatter.11.cloned.1.call-update) | async-done | bytes 65552 | tf_op jit(solution)/shard_map/reduce_scatter | solution.py:56
  52.9 20.5 %reduce-scatter.9.cloned.1.call-done = f32[32,512]{1,0:T(8,128)} async-done(((f32[128,512]{1,0:T(8,128)}), f32[32,512]{1,0:T(8,128)}) %reduce-scatter.9.cloned.1.call-update) | async-done | bytes 65552 | tf_op jit(solution)/shard_map/reduce_scatter | solution.py:59
  73.5 1.0 fusion.25
  74.5 0.1 reshape.83
  74.6 0.1 reshape.82
  74.7 0.1 reshape.86
  74.8 0.1 exponential_multiply_fusion
  75.0 9.7 %fusion.1 = bf16[32,16,256]{2,1,0:T(8,128)(2,1)S(1)} fusion(f32[32,16,32]{2,1,0:T(8,128)S(1)} %reshape.83, f32[32,16,32]{2,1,0:T(8,128)S(1)} %reshape.82, pred[32,256]{1,0:T(8,128)(4,1)S(1)} %iota_compare_fusion, bf16[32,512,256]{2,1,0:T(8,128)(2,1)} %param.21, f32[32,512,256]{2,1,0:T(8,128)} %param.23), kind=kLoop, calls=%fused_computation.2 | loop fusion | flops 25034752 | bytes 25567232 | tf_op jit(solution)/shard_map/reduce_sum | solution.py:80
  84.7 10.3 %fusion.8 = f32[32,16,1,64]{3,2,1,0:T(1,128)S(1)} fusion(bf16[32,16,64,256]{3,2,1,0:T(8,128)(2,1)} %bitcast.34, bf16[32,16,256,1]{2,1,0,3:T(8,128)(2,1)S(1)} %bitcast.32), kind=kOutput, calls=%fused_computation.16 | convolution fusion | flops 16777216 | bytes 17170432 | tf_op jit(solution)/shard_map/nhs,nhvs->nhv/dot_general | solution.py:83
  94.9 9.2 %fusion.29 = f32[32,16,1,64]{3,2,1,0:T(1,128)S(1)} fusion(f32[32,16,32,1]{2,3,1,0:T(1,128)S(1)} %bitcast.31, f32[32,16,32,64]{3,2,1,0:T(8,128)} %param.20), kind=kOutput, calls=%fused_computation.49 | convolution fusion | flops 12582912 | bytes 4390912 | tf_op jit(solution)/shard_map/nhc,nhcv->nhv/dot_general | solution.py:86
  104.2 0.0 reduce-scatter.13.cloned.1.call-done
  104.2 1.0 broadcast_multiply_fusion
  105.2 0.1 reshape.87
  105.3 0.2 multiply_reduce_fusion
  105.6 0.1 multiply_multiply_fusion
  105.7 0.1 reshape.88
  105.8 12.1 %reduce-scatter.15.cloned.1.call-done = f32[32,1024]{1,0:T(8,128)} async-done(((f32[128,1024]{1,0:T(8,128)}), f32[32,1024]{1,0:T(8,128)}) %reduce-scatter.15.cloned.1.call-update) | async-done | bytes 131088 | tf_op jit(solution)/shard_map/reduce_scatter | solution.py:58
  118.0 1.0 multiply_convert_fusion.1
  119.0 14.0 %all_gather.6 = bf16[128,1024]{1,0:T(8,128)(2,1)S(1)} all-gather(bf16[32,1024]{1,0:T(8,128)(2,1)S(1)} %multiply_convert_fusion.1), channel_id=1, replica_groups=mesh['grp'=2,'kv'=4,'tp'=4] {'kv'}, dimensions={0}, use_global_device_ids=true | all-gather | bytes 327680 | tf_op jit(solution)/shard_map/all_gather | solution.py:94
  133.0 0.4 fusion.30
  133.4 0.1 collective-permute-start
  133.5 1.9 collective-permute-done
  135.4 0.1 add.91
  135.5 1.5 collective-permute-start.1
  137.0 12.5 %collective-permute-done.1 = f32[128,1024]{1,0:T(8,128)S(1)} collective-permute-done((f32[128,1024]{1,0:T(8,128)S(1)}, f32[128,1024]{1,0:T(8,128)S(1)}, u32[]{:S(2)}, u32[]{:S(2)}) %collective-permute-start.1) | collective-permute-done | bytes 524320 | tf_op jit(solution)/shard_map/ppermute | solution.py:17
  149.5 0.2 fusion.6
  149.7 6.0 %fusion.10 = f32[128,4096]{1,0:T(8,128)} fusion(bf16[1024,4096]{1,0:T(8,128)(2,1)} %param.34, bf16[128,1024]{1,0:T(8,128)(2,1)S(1)} %get-tuple-element.6, f32[1024]{0:T(1024)S(1)} %copy-done.5), kind=kOutput, calls=%fused_computation.19 | convolution fusion | flops 1074135040 | bytes 10752000 | tf_op jit(solution)/shard_map/dot_general | solution.py:103
  155.7 0.0 reduce-scatter.17.cloned.1.call-update
  155.7 0.0 all-gather.2.cloned.1.call-start
  155.8 0.6 dynamic-slice
  157.0 9.0 %all-reduce = f32[128]{0:T(128)S(1)} all-reduce(f32[128]{0:T(128)S(1)} %get-tuple-element.5), channel_id=8, replica_groups=mesh['grp'=2,'kv'=4,'tp'=4] {'kv'}, use_global_device_ids=true, to_apply=%region_13.14.clone | all-reduce | flops 128 | bytes 1024
  166.0 0.1 fusion.27
  166.1 31.6 %reduce-scatter.17.cloned.1.call-done = f32[32,4096]{1,0:T(8,128)} async-done(((f32[128,4096]{1,0:T(8,128)}), f32[32,4096]{1,0:T(8,128)}) %reduce-scatter.17.cloned.1.call-update) | async-done | bytes 524304 | tf_op jit(solution)/shard_map/reduce_scatter | solution.py:105
  197.7 1.9 multiply_convert_fusion
  199.6 0.0 all-gather.2.cloned.1.call-update
  199.6 0.0 all-reduce.3.cloned.1.call-start
  199.6 27.3 %all-gather.2.cloned.1.call-done = bf16[128,4096]{1,0:T(8,128)(2,1)} async-done(((bf16[32,4096]{1,0:T(8,128)(2,1)}), bf16[128,4096]{1,0:T(8,128)(2,1)}) %all-gather.2.cloned.1.call-update) | async-done | bytes 1048592 | tf_op jit(solution)/shard_map/all_gather | solution.py:113
  226.9 5.8 %fusion.31 = f32[128,1024]{1,0:T(8,128)} fusion(bf16[128,4096]{1,0:T(8,128)(2,1)} %all-gather.2.cloned.1.call-done, bf16[4096,1024]{1,0:T(8,128)(2,1)} %param.35), kind=kOutput, calls=%fused_computation.51 | convolution fusion | flops 1073741824 | bytes 9961472 | tf_op jit(solution)/shard_map/dot_general | solution.py:112
  232.7 0.0 all-reduce.3.cloned.1.call-update
  232.7 32.9 %all-reduce.3.cloned.1.call-done = f32[128,1024]{1,0:T(8,128)} async-done(((f32[128,1024]{1,0:T(8,128)}), f32[128,1024]{1,0:T(8,128)}) %all-reduce.3.cloned.1.call-update) | async-done | bytes 524304 | tf_op jit(solution)/shard_map/psum | solution.py:117
  265.7 1.8 fusion.7
  (22 shorter events, 0.1 us)
Async XLA Ops:
  6.5 7.5 %copy-start = (bf16[1024,1024]{1,0:T(8,128)(2,1)S(1)}, bf16[1024,1024]{1,0:T(8,128)(2,1)}, u32[]{:S(2)}) copy-start(bf16[1024,1024]{1,0:T(8,128)(2,1)} %param.27) | copy-start | bytes 6291460
  6.5 9.8 %copy-start.2 = (bf16[128,1024]{1,0:T(8,128)(2,1)S(1)}, bf16[128,1024]{1,0:T(8,128)(2,1)}, u32[]{:S(2)}) copy-start(bf16[128,1024]{1,0:T(8,128)(2,1)} %param.18) | copy-start | bytes 786436
  6.5 9.8 %copy-start.4 = (f32[1024]{0:T(1024)S(1)}, f32[1024]{0:T(1024)}, u32[]{:S(2)}) copy-start(f32[1024]{0:T(1024)} %param.24) | copy-start | bytes 12292
  6.5 26.4 %copy-start.8 = (s32[32]{0:T(128)S(1)}, s32[32]{0:T(128)}, u32[]{:S(2)}) copy-start(s32[32]{0:T(128)} %param.19) | copy-start | bytes 388
  6.5 34.7 %reduce-scatter.7.cloned.1.call-start = ((), (), s32[]{:S(2)}) async-start(), calls=%async_computation.6 | async-start | bytes 327680 | tf_op jit(solution)/shard_map/reduce_scatter | solution.py:55
  9.1 43.8 %reduce-scatter.11.cloned.1.call-start = ((), (), s32[]{:S(2)}) async-start(), calls=%async_computation.8 | async-start | bytes 327680 | tf_op jit(solution)/shard_map/reduce_scatter | solution.py:56
  11.5 61.9 %reduce-scatter.9.cloned.1.call-start = ((), (), s32[]{:S(2)}) async-start(), calls=%async_computation.7 | async-start | bytes 327680 | tf_op jit(solution)/shard_map/reduce_scatter | solution.py:59
  14.0 90.2 %reduce-scatter.13.cloned.1.call-start = ((), (), s32[]{:S(2)}) async-start(), calls=%async_computation.9 | async-start | bytes 655360 | tf_op jit(solution)/shard_map/reduce_scatter | solution.py:57
  16.2 101.7 %reduce-scatter.15.cloned.1.call-start = ((), (), s32[]{:S(2)}) async-start(), calls=%async_computation.10 | async-start | bytes 655360 | tf_op jit(solution)/shard_map/reduce_scatter | solution.py:58
  19.2 178.5 %reduce-scatter.17.cloned.1.call-start = ((), (), s32[]{:S(2)}) async-start(), calls=%async_computation.11 | async-start | bytes 2621440 | tf_op jit(solution)/shard_map/reduce_scatter | solution.py:105
  33.2 40.2 %copy-start.6 = (f32[512]{0:T(512)S(1)}, f32[512]{0:T(512)}, u32[]{:S(2)}) copy-start(f32[512]{0:T(512)} %param.30) | copy-start | bytes 6148
  94.9 10.6 %copy-start.7 = (f32[64]{0:T(128)S(1)}, f32[64]{0:T(128)}, u32[]{:S(2)}) copy-start(f32[64]{0:T(128)} %param.31) | copy-start | bytes 772
  94.9 38.0 %copy-start.3 = (bf16[1024,1024]{1,0:T(8,128)(2,1)S(1)}, bf16[1024,1024]{1,0:T(8,128)(2,1)}, u32[]{:S(2)}) copy-start(bf16[1024,1024]{1,0:T(8,128)(2,1)} %param.32) | copy-start | bytes 6291460
  94.9 54.7 %copy-start.5 = (f32[1024]{0:T(1024)S(1)}, f32[1024]{0:T(1024)}, u32[]{:S(2)}) copy-start(f32[1024]{0:T(1024)} %param.33) | copy-start | bytes 12292
  133.4 2.0 collective-permute-start
  135.5 14.0 %collective-permute-start.1 = (f32[128,1024]{1,0:T(8,128)S(1)}, f32[128,1024]{1,0:T(8,128)S(1)}, u32[]{:S(2)}, u32[]{:S(2)}) collective-permute-start(f32[128,1024]{1,0:T(8,128)S(1)} %add.91), channel_id=1, source_target_pairs={{0,2},{1,3},{2,0},{3,1},{4,6},{5,7},{6,4},{7,5},{8,10},{9,11},{10,... | collective-permute-start | bytes 1572872 | tf_op jit(solution)/shard_map/ppermute | solution.py:17
  149.7 6.1 %copy-start.9 = (u32[32]{0:T(128)S(1)}, u32[32]{0:T(128)}, u32[]{:S(2)}) copy-start(u32[32]{0:T(128)} %constant.44) | copy-start | bytes 388
  155.7 71.2 %all-gather.2.cloned.1.call-start = ((), (), s32[]{:S(2)}) async-start(), calls=%async_computation.12 | async-start | bytes 1310720 | tf_op jit(solution)/shard_map/all_gather | solution.py:113
  199.6 67.9 %copy-start.1 = (bf16[1024,1024]{1,0:T(8,128)(2,1)S(1)}, bf16[1024,1024]{1,0:T(8,128)(2,1)}, u32[]{:S(2)}) copy-start(bf16[1024,1024]{1,0:T(8,128)(2,1)} %param.27) | copy-start | bytes 6291460
  199.6 66.1 %all-reduce.3.cloned.1.call-start = ((), (), s32[]{:S(2)}) async-start(), calls=%async_computation.13 | async-start | bytes 1048576 | tf_op jit(solution)/shard_map/psum | solution.py:117
Sparse Core Ops, SparseCore 0:
  9.6 22.7 reduce-scatter.6
  34.6 18.2 reduce-scatter.10
  55.2 18.2 reduce-scatter.8
  75.6 20.1 reduce-scatter.12
  97.8 20.0 reduce-scatter.14
  155.8 41.8 reduce-scatter.16
  199.7 27.1 all-gather.1
  232.9 32.7 all-reduce.2
